TPU v7x, 32 devices: a whole 2x2x4 slice. The times are simulated.
32 devices in a mesh: grp: 2 (over x), ep: 16 (over z, y, core).
Axes of the slice: x: 2, y: 2, z: 4, core: 2. Of those that a mesh axis runs over, the one named last changes fastest.
Arguments:
- stream: bfloat16 [32, 2048], P('grp', 'ep'), parts along dimension 0, may hold values from -48 to 48
- conv_cache: bfloat16 [32, 3, 2560], P(('grp', 'ep')), parts along dimension 0, may hold values from -6 to 6
- scan_state: float32 [32, 32, 64, 128], P(('grp', 'ep')), parts along dimension 0, may hold values from -4 to 4
- gate_weight: bfloat16 [2048, 2048], P('ep'), may hold values from -0.125 to 0.125
- value_weight: bfloat16 [2048, 2048], P('ep'), may hold values from -0.125 to 0.125
- entry_weight: bfloat16 [2048, 256], P('ep'), may hold values from -0.125 to 0.125
- readout_weight: bfloat16 [2048, 256], P('ep'), may hold values from -0.125 to 0.125
- step_weight: bfloat16 [2048, 32], P('ep'), may hold values from -0.125 to 0.125
- conv_weight: bfloat16 [4, 2560], replicated, may hold values from -3 to 3
- step_bias: float32 [32], replicated, may hold values from -4 to -1
- decay_rate: float32 [32], replicated, may hold values from 0.5 to 8
- skip_gain: float32 [32], replicated, may hold values from 0.1 to 1.9
- group_gain: float32 [2048], replicated, may hold values from 0.1 to 1.9
- out_weight: bfloat16 [2048, 2048], P(None, 'ep'), may hold values from -0.125 to 0.125
- first_gain: float32 [2048], replicated, may hold values from 0.1 to 1.9
- routes: int32 [32, 4], P('grp'), parts along dimension 0, may hold values from 0 to 15, all different within a row; in each aligned block of 16 rows (0 to 15, 16 to 31, ...) at most 8 rows name the same one
- route_weight: float32 [32, 4], P('grp'), parts along dimension 0, may hold values from 0.1 to 1
- expert_gate: bfloat16 [16, 2048, 256], P('ep'), may hold values from -0.125 to 0.125
- expert_up: bfloat16 [16, 2048, 256], P('ep'), may hold values from -0.125 to 0.125
- expert_down: bfloat16 [16, 256, 2048], P('ep'), may hold values from -0.375 to 0.375
- shared_gate: bfloat16 [2048, 256], replicated, may hold values from -0.125 to 0.125
- shared_up: bfloat16 [2048, 256], replicated, may hold values from -0.125 to 0.125
- shared_down: bfloat16 [256, 2048], replicated, may hold values from -0.375 to 0.375
- second_gain: float32 [2048], P('ep'), may hold values from 0.1 to 1.9
Outputs:
- result: bfloat16 [32, 2048], P('grp', 'ep'), parts along dimension 0
- new_conv: bfloat16 [32, 3, 2560], P(('grp', 'ep')), parts along dimension 0
- new_state: float32 [32, 32, 64, 128], P(('grp', 'ep')), parts along dimension 0
There are 2 independent parts, one for each index of `grp`. A program takes and returns all parts, laid end to end along the dimension named above; an argument that names none is the same for every part. Nothing has to cross between parts.
Inputs may be any that keep to these rules, and one draw needn't show every extreme that they name: `routes`: each row names 4 different experts; no expert is named by more than 8 rows, a bound that some block reaches.
All inputs are finite; a program needn't handle non-finite values.
Results may differ from a plain program's by a relative error of at most 0.0065.
Values may be sent and summed in bfloat16 or wider, within the bound.
A program may use at most 64 MiB of HBM per device.

v0:
```python
import jax
import jax.numpy as jnp
from jax import lax
from jax.sharding import PartitionSpec as P

HEAD_DIM = 64
STATE = 128
GROUPS = 2
CAP = 8


RESIDUAL_SCALE = 2.0**0.25
NORM_EPSILON = 1e-05
GATED_EPSILON = 1e-06


def rounded(value):
    return lax.optimization_barrier(value.astype(jnp.bfloat16))


def finish_norm(residual, row_total, square, full_width, gain):
    mean_value = (row_total / full_width)[:, None]
    variance = (square / full_width)[:, None] - mean_value * mean_value
    return (residual - mean_value) * lax.rsqrt(variance + NORM_EPSILON) * gain


def swiglu(inputs, gate_matrix, up_matrix, down_matrix):
    hidden = (
        jax.nn.silu(jnp.dot(inputs, gate_matrix, preferred_element_type=jnp.float32))
        * jnp.dot(inputs, up_matrix, preferred_element_type=jnp.float32)
    ).astype(jnp.bfloat16)
    return rounded(jnp.dot(hidden, down_matrix, preferred_element_type=jnp.float32))


def on_device(
    stream,
    conv_cache,
    scan_state,
    gate_weight,
    value_weight,
    entry_weight,
    readout_weight,
    step_weight,
    conv_weight,
    step_bias,
    decay_rate,
    skip_gain,
    group_gain,
    out_weight,
    first_gain,
    routes,
    route_weight,
    expert_gate,
    expert_up,
    expert_down,
    shared_gate,
    shared_up,
    shared_down,
    second_gain,
):
    devices = lax.axis_size("ep")
    device_rank = lax.axis_index("ep")
    own_rows = conv_cache.shape[0]
    row_count = stream.shape[0]
    slice_width = stream.shape[1]
    full_width = slice_width * devices
    inner_width = gate_weight.shape[1]
    head_count = step_weight.shape[1]
    per_group = head_count // GROUPS
    group_width = inner_width // GROUPS
    bounds = (inner_width, 2 * inner_width + 2 * GROUPS * STATE)
    weights_in = (gate_weight, value_weight, entry_weight, readout_weight, step_weight)
    summed = rounded(
        lax.psum_scatter(
            jnp.concatenate(
                [
                    jnp.dot(stream, weight, preferred_element_type=jnp.float32)
                    for weight in weights_in
                ],
                axis=1,
            ),
            "ep",
            scatter_dimension=0,
            tiled=True,
        )
    )
    gate_rows = summed[:, : bounds[0]]
    fresh = summed[:, bounds[0] : bounds[1]]
    step_rows = summed[:, bounds[1] :]
    window = jnp.concatenate([conv_cache, fresh[:, None, :]], axis=1)
    active = jax.nn.silu(
        jnp.sum(window.astype(jnp.float32) * conv_weight.astype(jnp.float32)[None], axis=1)
    )
    head_in = active[:, :inner_width].reshape(own_rows, GROUPS, per_group, HEAD_DIM)
    entry_rows = active[:, inner_width : inner_width + GROUPS * STATE].reshape(
        own_rows, GROUPS, 1, 1, STATE
    )
    readout_rows = active[:, inner_width + GROUPS * STATE :].reshape(own_rows, GROUPS, 1, 1, STATE)
    step_size = jax.nn.softplus(step_rows.astype(jnp.float32) + step_bias).reshape(
        own_rows, GROUPS, per_group
    )
    retained = jnp.exp(-step_size * decay_rate.reshape(GROUPS, per_group))
    old_state = scan_state.reshape(own_rows, GROUPS, per_group, HEAD_DIM, STATE)
    new_state = (
        retained[..., None, None] * old_state
        + (step_size[..., None] * head_in)[..., None] * entry_rows
    )
    head_out = (
        jnp.sum(new_state * readout_rows, axis=-1)
        + skip_gain.reshape(GROUPS, per_group)[:, :, None] * head_in
    )
    gated_out = head_out.reshape(own_rows, GROUPS, group_width) * jax.nn.silu(
        gate_rows.astype(jnp.float32)
    ).reshape(own_rows, GROUPS, group_width)
    normed = gated_out * lax.rsqrt(
        jnp.mean(gated_out * gated_out, axis=-1, keepdims=True) + GATED_EPSILON
    )
    normed = (normed.reshape(own_rows, inner_width) * group_gain).astype(jnp.bfloat16)
    mixer_out = rounded(
        jnp.dot(
            lax.all_gather(normed, "ep", axis=0, tiled=True),
            out_weight,
            preferred_element_type=jnp.float32,
        )
    )
    column_start = device_rank * slice_width
    residual = RESIDUAL_SCALE * stream.astype(jnp.float32) + mixer_out.astype(jnp.float32)
    row_total, square = lax.psum(
        (jnp.sum(residual, axis=1), jnp.sum(residual * residual, axis=1)), "ep"
    )
    gain_part = lax.dynamic_slice_in_dim(first_gain, column_start, slice_width, 0)
    first_part = rounded(finish_norm(residual, row_total, square, full_width, gain_part))
    first_rows = lax.all_gather(first_part, "ep", axis=1, tiled=True)
    matches = routes[:, :, None] == jnp.arange(devices, dtype=jnp.int32)[None, None, :]
    member = jnp.sum(matches.astype(jnp.int32), axis=1)
    weight_of = jnp.sum(jnp.where(matches, route_weight[:, :, None], 0.0), axis=1)
    slot_rank = jnp.cumsum(member, axis=0) - member
    slot_ids = jnp.arange(CAP, dtype=jnp.int32)
    mine_member = lax.dynamic_slice_in_dim(member, device_rank, 1, 1)[:, 0]
    mine_slot = lax.dynamic_slice_in_dim(slot_rank, device_rank, 1, 1)[:, 0]
    chosen = (mine_slot[None, :] == slot_ids[:, None]) & (mine_member[None, :] == 1)
    taken_rows = jnp.dot(
        chosen.astype(jnp.bfloat16), first_rows, preferred_element_type=jnp.float32
    ).astype(jnp.bfloat16)
    expert_out = swiglu(taken_rows, expert_gate[0], expert_up[0], expert_down[0])
    arrived = lax.all_to_all(expert_out, "ep", split_axis=1, concat_axis=0, tiled=True)
    spread = jnp.where(
        (slot_rank[:, :, None] == slot_ids[None, None, :]) & (member[:, :, None] == 1),
        weight_of[:, :, None],
        0.0,
    )
    moe_part = jnp.dot(
        spread.reshape(row_count, devices * CAP),
        arrived.astype(jnp.float32),
        precision=lax.Precision.HIGHEST,
    )
    down_part = lax.dynamic_slice_in_dim(shared_down, column_start, slice_width, 1)
    shared_part = swiglu(first_rows, shared_gate, shared_up, down_part)
    moe_part = moe_part + shared_part.astype(jnp.float32)
    residual_two = RESIDUAL_SCALE * first_part.astype(jnp.float32) + moe_part
    total_two, square_two = lax.psum(
        (jnp.sum(residual_two, axis=1), jnp.sum(residual_two * residual_two, axis=1)), "ep"
    )
    result = finish_norm(residual_two, total_two, square_two, full_width, second_gain).astype(
        jnp.bfloat16
    )
    return (result, window[:, 1:], new_state.reshape(own_rows, head_count, HEAD_DIM, STATE))


def solution(mesh):
    return jax.shard_map(
        on_device,
        mesh=mesh,
        in_specs=(
            P("grp", "ep"),
            P(("grp", "ep"), None, None),
            P(("grp", "ep"), None, None, None),
            P("ep", None),
            P("ep", None),
            P("ep", None),
            P("ep", None),
            P("ep", None),
            P(),
            P(),
            P(),
            P(),
            P(),
            P(None, "ep"),
            P(),
            P("grp", None),
            P("grp", None),
            P("ep", None, None),
            P("ep", None, None),
            P("ep", None, None),
            P(),
            P(),
            P(),
            P("ep"),
        ),
        out_specs=(
            P("grp", "ep"),
            P(("grp", "ep"), None, None),
            P(("grp", "ep"), None, None, None),
        ),
        check_vma=False,
    )
```

profile of v0, /device:TPU:0, one launch (start us, length us, event | category | flops | bytes accessed | tf_op | source)
XLA Modules:
  0.0 191.0 jit_solution(8677031213126030681)
XLA Ops:
  0.7 0.7 copy-done.7
  1.4 1.3 convolution_dynamic-update-slice_fusion.1
  2.7 0.2 convolution_dynamic-update-slice_fusion
  2.9 1.0 convolution_dynamic-update-slice_fusion.3
  3.9 1.0 convolution_dynamic-update-slice_fusion.2
  4.9 0.8 convolution_dynamic-update-slice_fusion.4
  5.7 66.2 %all-reduce.4 = bf16[16,4640]{1,0:T(8,128)(2,1)S(1)} all-reduce(f32[16,4640]{1,0:T(8,128)S(1)} %convolution_dynamic-update-slice_fusion.4), channel_id=3, replica_groups=mesh['grp'=2,'ep'=16] {'ep'}, use_global_device_ids=true, to_apply=%region_0.0.clone | all-reduce | flops 74240 | bytes 445440
  71.9 0.6 copy-done.17
  72.6 0.6 dynamic-slice
  73.1 0.7 dynamic-slice_convert_fusion
  73.9 0.7 copy-done.8
  74.8 0.6 copy-done.14
  75.5 1.4 multiply_reduce_fusion
  77.4 0.5 broadcast.167
  77.9 0.7 fusion.47
  78.8 17.3 %all-gather = bf16[32768]{0:T(1024)(128)(2,1)S(1)} all-gather(bf16[2048]{0:T(1024)(128)(2,1)S(1)} %multiply_convert_fusion.2), channel_id=2, replica_groups=mesh['grp'=2,'ep'=16] {'ep'}, dimensions={0}, use_global_device_ids=true | all-gather | bytes 69632 | tf_op jit(solution)/shard_map/all_gather | solution.py:121
  96.2 1.3 convolution_convert_fusion.2
  97.6 0.8 dynamic_slice.12
  98.4 31.4 %all-reduce.2 = (f32[16]{0:T(128)S(1)}, f32[16]{0:T(128)S(1)}) all-reduce(f32[16]{0:T(128)S(1)} %get-tuple-element.6, f32[16]{0:T(128)S(1)} %get-tuple-element.5), channel_id=1, replica_groups=mesh['grp'=2,'ep'=16] {'ep'}, use_global_device_ids=true, to_apply=%region_7.8 | all-reduce | flops 32 | bytes 256 | tf_op jit(solution)/shard_map/psum | solution.py:128
  129.9 17.3 %all_gather.7 = bf16[16,2048]{1,0:T(8,128)(2,1)S(1)} all-gather(bf16[16,128]{1,0:T(8,128)(2,1)S(1)} %multiply_convert_fusion.1), channel_id=1, replica_groups=mesh['grp'=2,'ep'=16] {'ep'}, dimensions={1}, use_global_device_ids=true | all-gather | bytes 69632 | tf_op jit(solution)/shard_map/all_gather | solution.py:133
  147.3 0.2 fusion.32
  147.8 0.2 fusion.9
  148.1 1.3 convolution_convert_fusion
  149.4 3.6 %all-to-all-start = ((bf16[8,16,128]{2,0,1:T(8,128)(2,1)}), bf16[8,16,128]{2,0,1:T(8,128)(2,1)S(1)}, u32[]{:S(2)}, u32[]{:S(2)}) async-start(bf16[8,16,128]{2,0,1:T(8,128)(2,1)} %bitcast.13), calls=%async_computation | async-start | bytes 65536 | tf_op jit(solution)/shard_map/all_to_all | solution.py:146
  153.0 0.2 fusion.50
  153.3 1.2 fusion.5
  154.5 0.7 pad_maximum_fusion
  155.3 4.3 %all-to-all-done = bf16[8,16,128]{2,0,1:T(8,128)(2,1)S(1)} async-done(((bf16[8,16,128]{2,0,1:T(8,128)(2,1)}), bf16[8,16,128]{2,0,1:T(8,128)(2,1)S(1)}, u32[]{:S(2)}, u32[]{:S(2)}) %all-to-all-start) | async-done | bytes 32800 | tf_op jit(solution)/shard_map/all_to_all | solution.py:146
  159.6 0.4 fusion.45
  160.0 29.7 %all-reduce.1 = (f32[16]{0:T(128)S(1)}, f32[16]{0:T(128)S(1)}) all-reduce(f32[16]{0:T(128)S(1)} %get-tuple-element.4, f32[16]{0:T(128)S(1)} %get-tuple-element.3), channel_id=1, replica_groups=mesh['grp'=2,'ep'=16] {'ep'}, use_global_device_ids=true, to_apply=%region_14.15 | all-reduce | flops 32 | bytes 256 | tf_op jit(solution)/shard_map/psum | solution.py:161
  189.7 0.7 copy-done.13
  190.3 0.7 multiply_convert_fusion
  (65 shorter events, 1.9 us)
Async XLA Ops:
  0.6 147.4 %copy-start = (bf16[1,256,2048]{2,1,0:T(8,128)(2,1)S(1)}, bf16[1,256,2048]{2,1,0:T(8,128)(2,1)}, u32[]{:S(2)}) copy-start(bf16[1,256,2048]{2,1,0:T(8,128)(2,1)} %param.43) | copy-start | bytes 3145732
  0.6 0.8 copy-start.7
  0.7 2.1 %copy-start.6 = (bf16[128,2048]{1,0:T(8,128)(2,1)S(1)}, bf16[128,2048]{1,0:T(8,128)(2,1)}, u32[]{:S(2)}) copy-start(bf16[128,2048]{1,0:T(8,128)(2,1)} %param.28) | copy-start | bytes 1572868
  1.4 74.1 %copy-start.1 = (f32[1,32,64,128]{3,2,1,0:T(8,128)S(1)}, f32[1,32,64,128]{3,2,1,0:T(8,128)}, u32[]{:S(2)}) copy-start(f32[1,32,64,128]{3,2,1,0:T(8,128)} %param.26) | copy-start | bytes 3145732
  71.9 0.7 copy-start.17
  73.1 0.7 copy-start.9
  73.8 0.7 copy-start.8
  74.7 0.7 copy-start.14
  74.7 0.7 copy-start.15
  75.5 1.6 copy-start.16
  75.5 3.3 %copy-start.11 = (f32[2048]{0:T(1024)S(1)}, f32[2048]{0:T(1024)}, u32[]{:S(2)}) copy-start(f32[2048]{0:T(1024)} %param.36) | copy-start | bytes 24580
  76.9 70.9 %copy-start.2 = (bf16[1,2048,256]{2,1,0:T(8,128)(2,1)S(1)}, bf16[1,2048,256]{2,1,0:T(8,128)(2,1)}, u32[]{:S(2)}) copy-start(bf16[1,2048,256]{2,1,0:T(8,128)(2,1)} %param.41) | copy-start | bytes 3145732
  78.8 68.3 %copy-start.10 = (s32[16,4]{0,1:T(4,128)S(1)}, s32[16,4]{0,1:T(4,128)}, u32[]{:S(2)}) copy-start(s32[16,4]{0,1:T(4,128)} %param.39) | copy-start | bytes 772
  96.1 51.9 %copy-start.3 = (bf16[1,2048,256]{2,1,0:T(8,128)(2,1)S(1)}, bf16[1,2048,256]{2,1,0:T(8,128)(2,1)}, u32[]{:S(2)}) copy-start(bf16[1,2048,256]{2,1,0:T(8,128)(2,1)} %param.42) | copy-start | bytes 3145732
  148.0 5.0 %copy-start.4 = (bf16[2048,256]{1,0:T(8,128)(2,1)S(1)}, bf16[2048,256]{1,0:T(8,128)(2,1)}, u32[]{:S(2)}) copy-start(bf16[2048,256]{1,0:T(8,128)(2,1)} %param.44) | copy-start | bytes 3145732
  149.4 3.9 %copy-start.5 = (bf16[2048,256]{1,0:T(8,128)(2,1)S(1)}, bf16[2048,256]{1,0:T(8,128)(2,1)}, u32[]{:S(2)}) copy-start(bf16[2048,256]{1,0:T(8,128)(2,1)} %param.45) | copy-start | bytes 3145732
  149.4 10.2 %all-to-all-start = ((bf16[8,16,128]{2,0,1:T(8,128)(2,1)}), bf16[8,16,128]{2,0,1:T(8,128)(2,1)S(1)}, u32[]{:S(2)}, u32[]{:S(2)}) async-start(bf16[8,16,128]{2,0,1:T(8,128)(2,1)} %bitcast.13), calls=%async_computation | async-start | bytes 65536 | tf_op jit(solution)/shard_map/all_to_all | solution.py:146
  154.5 0.7 copy-start.12
  189.7 0.7 copy-start.13
where the time goes:
time: 192 us; the launch traced here: 191 us
  blocking collectives  162 us (84%)
  matrix products  9.08 us (5%)
  local copies, waits for them, and re-layouts  6.89 us (4%)
  waiting for transfers between devices  4.33 us (2%)
  other arithmetic  4.32 us (2%)
  starting transfers between devices  3.63 us (2%)
    unnamed x1, blocking collectives  66.2 us
    psum x1, blocking collectives, on_device(): lax.psum((jnp.sum(residual, axis=1), jnp.sum(residual * residual, axis=1)...  31.4 us
    psum x1, blocking collectives, on_device(): lax.psum((jnp.sum(residual_two, axis=1), jnp.sum(residual_two * residual_...  29.7 us
    all_gather x1, blocking collectives, on_device(): lax.all_gather(normed, 'ep', axis=0, tiled=True)  17.3 us
    all_gather x1, blocking collectives, on_device(): first_rows = lax.all_gather(first_part, 'ep', axis=1, tiled=True)  17.3 us
    all_to_all x1, waiting for transfers between devices, on_device(): lax.all_to_all(expert_out, 'ep', split_axis=1, concat_axis=0, tiled=True)  4.33 us
    dot_general x5, matrix products, on_device(): jnp.dot(stream, weight, preferred_element_type=jnp.float32)  4.26 us
    unnamed x37, local copies, waits for them, and re-layouts  4.03 us
  transfers between devices with their start and end apart: 1, of which 1 were waited for; matrix products, arithmetic and copies ran while one was open for 1% of the time, Pallas kernels for 0%

commit v1 on v0

--- a/solution.py
+++ b/solution.py
@@ -1,6 +1,10 @@
+import functools
+
 import jax
 import jax.numpy as jnp
 from jax import lax
+from jax.experimental import pallas as pl
+from jax.experimental.pallas import tpu as pltpu
 from jax.sharding import PartitionSpec as P
 
 HEAD_DIM = 64
@@ -167,9 +171,475 @@
     return (result, window[:, 1:], new_state.reshape(own_rows, head_count, HEAD_DIM, STATE))
 
 
+MESH = pl.DeviceIdType.MESH
+LANES = 128
+ROWS = 40
+
+
+def silu(value):
+    return value * (1.0 / (1.0 + jnp.exp(-value)))
+
+
+def iota(shape, dim):
+    return lax.broadcasted_iota(jnp.int32, shape, dim)
+
+
+def fused_kernel(
+    sizes,
+    stream,
+    conv_cache,
+    scan_state,
+    gate_weight,
+    value_weight,
+    entry_weight,
+    readout_weight,
+    step_weight,
+    conv_weight,
+    step_bias,
+    decay_rate,
+    skip_gain,
+    group_gain,
+    out_weight,
+    first_gain,
+    routes,
+    route_weight,
+    expert_gate,
+    expert_up,
+    expert_down,
+    shared_gate,
+    shared_up,
+    shared_down,
+    second_gain,
+    result_ref,
+    conv_ref,
+    state_ref,
+    x_v,
+    cache_v,
+    state_v,
+    wg_v,
+    wv_v,
+    we_v,
+    wr_v,
+    ws_v,
+    cw_v,
+    sb_v,
+    dr_v,
+    sk_v,
+    gg_v,
+    ow_v,
+    fg_v,
+    rt_v,
+    rw_v,
+    eg_v,
+    eu_v,
+    ed_v,
+    sg_v,
+    su_v,
+    sd_v,
+    s2_v,
+    conv_v,
+    stage,
+    part_send,
+    part_recv,
+    x_recv,
+    norm_send,
+    norm_recv,
+    mix_send,
+    mix_recv,
+    out_send,
+    out_recv,
+    stat_send,
+    stat_recv,
+    taps,
+    past,
+    gains,
+    turn,
+    wide,
+    firsts,
+    load_sem,
+    store_sem,
+    send_sem,
+    recv_sem,
+):
+    n, inner, groups, head_dim = sizes
+    tokens = n
+    me = lax.axis_index("ep")
+    blocks = inner // LANES
+    heads_a_row = LANES // head_dim
+    heads = inner // head_dim
+    full_width = n * LANES
+    barrier = pltpu.get_barrier_semaphore()
+    for k in range(1, n):
+        pl.semaphore_signal(
+            barrier, inc=1, device_id={"ep": lax.rem(me + k, n)}, device_id_type=MESH
+        )
+
+    moves = (
+        (stream, x_v),
+        (step_weight, ws_v),
+        (gate_weight, wg_v),
+        (value_weight, wv_v),
+        (entry_weight, we_v),
+        (readout_weight, wr_v),
+        (conv_cache, cache_v),
+        (conv_weight, cw_v),
+        (step_bias, sb_v),
+        (decay_rate, dr_v),
+        (skip_gain, sk_v),
+        (group_gain, gg_v),
+        (routes, rt_v),
+        (route_weight, rw_v),
+        (first_gain, fg_v),
+        (second_gain, s2_v),
+        (scan_state.at[0], state_v),
+        (out_weight, ow_v),
+        (expert_gate.at[0], eg_v),
+        (expert_up.at[0], eu_v),
+        (expert_down.at[0], ed_v),
+        (shared_gate, sg_v),
+        (shared_up, su_v),
+        (shared_down.at[:, pl.ds(pl.multiple_of(me * LANES, LANES), LANES)], sd_v),
+    )
+    loads = {}
+    for index, (source, target) in enumerate(moves):
+        copy = pltpu.make_async_copy(source, target, load_sem.at[index])
+        copy.start()
+        loads[index] = copy
+
+    pending = []
+
+    def post(phase, source, target):
+        for k in range(1, n):
+            peer = lax.rem(me + k, n)
+            copy = pltpu.make_async_remote_copy(
+                src_ref=source(peer),
+                dst_ref=target.at[me],
+                send_sem=send_sem.at[phase, k],
+                recv_sem=recv_sem.at[phase, n - k],
+                device_id={"ep": peer},
+                device_id_type=MESH,
+            )
+            copy.start()
+            pending.append(copy)
+
+    def arrive(phase, target, k):
+        sender = lax.rem(me + k, n)
+        pltpu.make_async_remote_copy(
+            src_ref=target.at[sender],
+            dst_ref=target.at[sender],
+            send_sem=send_sem.at[phase, k],
+            recv_sem=recv_sem.at[phase, k],
+            device_id={"ep": sender},
+            device_id_type=MESH,
+        ).wait_recv()
+        return sender
+
+    for index in range(2):
+        loads[index].wait()
+    x = x_v[...]
+    place = (iota((heads, LANES), 0) == iota((heads, LANES), 1)).astype(jnp.bfloat16)
+    step_wide = jnp.dot(ws_v[...], place, preferred_element_type=jnp.float32).astype(jnp.bfloat16)
+    base = 2 * blocks + 2 * groups
+    stage[pl.ds(base, tokens, stride=ROWS), :] = jnp.dot(
+        x, step_wide, preferred_element_type=jnp.float32
+    )
+    for extra in range(base + 1, ROWS):
+        stage[pl.ds(extra, tokens, stride=ROWS), :] = jnp.zeros((tokens, LANES), jnp.float32)
+    base = 0
+    for index, ref in ((2, wg_v), (3, wv_v), (4, we_v), (5, wr_v)):
+        loads[index].wait()
+        product = jnp.dot(x, ref[...], preferred_element_type=jnp.float32)
+        for j in range(ref.shape[1] // LANES):
+            stage[pl.ds(base + j, tokens, stride=ROWS), :] = product[
+                :, j * LANES : (j + 1) * LANES
+            ]
+        base += ref.shape[1] // LANES
+    for t in range(tokens):
+        part_send[t] = stage[t * ROWS : (t + 1) * ROWS, :].astype(jnp.bfloat16)
+    pl.semaphore_wait(barrier, n - 1)
+    post(0, lambda peer: part_send.at[peer], part_recv)
+    post(1, lambda peer: x_v, x_recv)
+
+    for index in range(6, 16):
+        loads[index].wait()
+    old_rows = cache_v[0].astype(jnp.float32)
+    tap_rows = cw_v[...].astype(jnp.float32)
+    conv_blocks = tap_rows.shape[1] // LANES
+    tap_count = tap_rows.shape[0]
+    for j in range(conv_blocks):
+        cut = slice(j * LANES, (j + 1) * LANES)
+        taps[pl.ds(j, tap_count, stride=24), :] = tap_rows[:, cut]
+        past[pl.ds(j, tap_count - 1, stride=24), :] = old_rows[:, cut]
+    for j in range(blocks):
+        gains[j : j + 1, :] = gg_v[:, j * LANES : (j + 1) * LANES]
+    own_row = iota((blocks, heads), 1) // heads_a_row == iota((blocks, heads), 0)
+    own_lane = (
+        iota((heads, LANES), 0) % heads_a_row == iota((heads, LANES), 1) // head_dim
+    ).astype(jnp.float32)
+
+    def expand(row):
+        return jnp.dot(
+            jnp.where(own_row, jnp.broadcast_to(row, (blocks, heads)), 0.0),
+            own_lane,
+            precision=lax.Precision.HIGHEST,
+            preferred_element_type=jnp.float32,
+        )
+
+    bias_rows = expand(sb_v[...])
+    decay_rows = expand(dr_v[...])
+    skip_rows = expand(sk_v[...])
+    before = jnp.zeros((24, LANES), jnp.float32)
+    for tap in range(tap_count - 1):
+        before = before + past[tap * 24 : (tap + 1) * 24, :] * taps[tap * 24 : (tap + 1) * 24, :]
+    last_tap = taps[(tap_count - 1) * 24 : tap_count * 24, :]
+    loads[16].wait()
+
+    total = stage[pl.ds(pl.multiple_of(me * ROWS, ROWS), ROWS), :]
+    for k in range(1, n):
+        sender = arrive(0, part_recv, k)
+        total = total + part_recv[sender].astype(jnp.float32)
+    total = total.astype(jnp.bfloat16).astype(jnp.float32)
+    fresh = total[blocks : blocks + 24, :]
+    active = silu(before + fresh * last_tap)
+    head_in = active[:blocks, :]
+    step_row = total[2 * blocks + 2 * groups : 2 * blocks + 2 * groups + 1, :heads]
+    biased = expand(step_row) + bias_rows
+    step = jnp.maximum(biased, 0.0) + jnp.log1p(jnp.exp(-jnp.abs(biased)))
+    retained = jnp.exp(-step * decay_rows)
+    scaled_in = step * head_in
+    rows_a_group = blocks // groups
+    group_row = iota((blocks, 1), 0) // rows_a_group
+    entry = [active[blocks + g : blocks + g + 1, :] for g in range(groups)]
+    readout = [active[blocks + groups + g : blocks + groups + g + 1, :] for g in range(groups)]
+    lane = iota((LANES, LANES), 1)
+    columns = jnp.zeros((LANES, LANES), jnp.float32)
+    for r in range(blocks):
+        old = state_v[r * heads_a_row : (r + 1) * heads_a_row].reshape(LANES, LANES)
+        dots = jnp.sum(old * readout[r // rows_a_group], axis=1, keepdims=True)
+        columns = jnp.where(lane == r, dots, columns)
+    old_out = columns.T[:blocks, :]
+    cross = jnp.zeros((blocks, 1), jnp.float32)
+    for g in range(groups):
+        both = jnp.sum(entry[g] * readout[g], axis=1, keepdims=True)
+        cross = jnp.where(group_row == g, both, cross)
+    head_out = retained * old_out + scaled_in * cross + skip_rows * head_in
+    gated = head_out * silu(total[:blocks, :])
+    squares = jnp.sum(gated * gated, axis=1, keepdims=True)
+    inverse = jnp.zeros((blocks, 1), jnp.float32)
+    for g in range(groups):
+        square = jnp.sum(
+            jnp.where(group_row == g, squares, 0.0), axis=0, keepdims=True
+        ) / (rows_a_group * LANES)
+        inverse = jnp.where(group_row == g, lax.rsqrt(square + GATED_EPSILON), inverse)
+    normed = (gated * inverse * gains[...]).astype(jnp.bfloat16)
+    norm_send[...] = normed
+    post(2, lambda peer: norm_send, norm_recv)
+    norm_recv[me] = normed
+
+    turn[0:blocks, :] = scaled_in
+    turn[blocks : 2 * blocks, :] = retained
+    turn[2 * blocks :, :] = jnp.zeros((LANES - 2 * blocks, LANES), jnp.float32)
+    turned = turn[...].T
+    for r in range(blocks):
+        own = slice(r * heads_a_row, (r + 1) * heads_a_row)
+        old = state_v[own].reshape(LANES, LANES)
+        new = (
+            turned[:, blocks + r : blocks + r + 1] * old
+            + turned[:, r : r + 1] * entry[r // rows_a_group]
+        )
+        state_v[own] = new.reshape(heads_a_row, head_dim, LANES)
+    state_out = pltpu.make_async_copy(state_v, state_ref.at[0], store_sem.at[0])
+    state_out.start()
+    new_row = jnp.concatenate([fresh[j : j + 1, :] for j in range(conv_blocks)], axis=1)
+    conv_v[0] = jnp.concatenate([old_rows[1:, :], new_row], axis=0).astype(jnp.bfloat16)
+    conv_out = pltpu.make_async_copy(conv_v, conv_ref, store_sem.at[1])
+    conv_out.start()
+    for index in range(17, len(moves)):
+        loads[index].wait()
+    x_recv[me] = x
+    for k in range(1, n):
+        arrive(1, x_recv, k)
+
+    for k in range(1, n):
+        arrive(2, norm_recv, k)
+    for t in range(tokens):
+        wide[t * blocks : (t + 1) * blocks, :] = norm_recv[t].astype(jnp.float32)
+    every = jnp.concatenate(
+        [wide[pl.ds(r, tokens, stride=blocks), :].astype(jnp.bfloat16) for r in range(blocks)],
+        axis=1,
+    )
+    mixed = jnp.dot(every, ow_v[...], preferred_element_type=jnp.float32).astype(jnp.bfloat16)
+    mix_send[...] = mixed
+    post(3, lambda peer: mix_send, mix_recv)
+    mix_recv[me] = mixed
+    mine = jnp.sum(jnp.where(rt_v[...] == me, rw_v[...], 0.0), axis=1, keepdims=True)
+    for k in range(1, n):
+        arrive(3, mix_recv, k)
+
+    residuals = [
+        RESIDUAL_SCALE * x_recv[d].astype(jnp.float32) + mix_recv[d].astype(jnp.float32)
+        for d in range(n)
+    ]
+    sums = residuals[0]
+    squares = residuals[0] * residuals[0]
+    for d in range(1, n):
+        sums = sums + residuals[d]
+        squares = squares + residuals[d] * residuals[d]
+    mean_value = jnp.sum(sums, axis=1, keepdims=True) / full_width
+    variance = jnp.sum(squares, axis=1, keepdims=True) / full_width - mean_value * mean_value
+    factor = lax.rsqrt(variance + NORM_EPSILON)
+    parts = []
+    for d in range(n):
+        part = (
+            (residuals[d] - mean_value) * factor * fg_v[:, d * LANES : (d + 1) * LANES]
+        ).astype(jnp.bfloat16)
+        firsts[d] = part
+        parts.append(part)
+    first_rows = jnp.concatenate(parts, axis=1)
+
+    def hidden(gate_ref, up_ref):
+        gate = jnp.dot(first_rows, gate_ref[...], preferred_element_type=jnp.float32)
+        up = jnp.dot(first_rows, up_ref[...], preferred_element_type=jnp.float32)
+        return (silu(gate) * up).astype(jnp.bfloat16)
+
+    routed = jnp.dot(hidden(eg_v, eu_v), ed_v[...], preferred_element_type=jnp.float32)
+    routed = (routed * mine).astype(jnp.bfloat16)
+    for d in range(n):
+        out_send[d] = routed[:, d * LANES : (d + 1) * LANES]
+    post(4, lambda peer: out_send.at[peer], out_recv)
+    shared = jnp.dot(hidden(sg_v, su_v), sd_v[...], preferred_element_type=jnp.float32)
+    shared = shared.astype(jnp.bfloat16).astype(jnp.float32)
+    moe = shared + out_send[me].astype(jnp.float32)
+    for k in range(1, n):
+        sender = arrive(4, out_recv, k)
+        moe = moe + out_recv[sender].astype(jnp.float32)
+    residual = RESIDUAL_SCALE * firsts[me].astype(jnp.float32) + moe
+
+    row_total = jnp.sum(residual, axis=1, keepdims=True)
+    row_square = jnp.sum(residual * residual, axis=1, keepdims=True)
+    token = iota((tokens, LANES), 0)
+    place = iota((tokens, LANES), 1)
+    compact = jnp.sum(
+        jnp.where(place == token, row_total, 0.0)
+        + jnp.where(place == token + tokens, row_square, 0.0),
+        axis=0,
+        keepdims=True,
+    )
+    stat_send[...] = compact
+    post(5, lambda peer: stat_send, stat_recv)
+    for k in range(1, n):
+        sender = arrive(5, stat_recv, k)
+        compact = compact + stat_recv[sender]
+    row_total = jnp.sum(jnp.where(place == token, compact, 0.0), axis=1, keepdims=True)
+    row_square = jnp.sum(jnp.where(place == token + tokens, compact, 0.0), axis=1, keepdims=True)
+    mean_value = row_total / full_width
+    variance = row_square / full_width - mean_value * mean_value
+    result_ref[...] = (
+        (residual - mean_value) * lax.rsqrt(variance + NORM_EPSILON) * s2_v[...]
+    ).astype(jnp.bfloat16)
+    for copy in pending:
+        copy.wait_send()
+    state_out.wait()
+    conv_out.wait()
+
+
+def fused(*arrays):
+    (stream, conv_cache, scan_state) = arrays[:3]
+    n = lax.axis_size("ep")
+    inner = arrays[3].shape[1]
+    groups = arrays[5].shape[1] // scan_state.shape[3]
+    blocks = inner // LANES
+    arrays = [a.reshape(1, -1) if a.ndim == 1 else a for a in arrays]
+    tile = (stream.shape[0], LANES)
+    landing = []
+    for index, a in enumerate(arrays):
+        shape = a.shape
+        if index in (2, 17, 18, 19):
+            shape = shape[1:]
+        if index == 22:
+            shape = (shape[0], LANES)
+        landing.append(pltpu.VMEM(shape, a.dtype))
+    bf16, f32 = jnp.bfloat16, jnp.float32
+    return pl.pallas_call(
+        functools.partial(fused_kernel, (n, inner, groups, scan_state.shape[2])),
+        out_shape=(
+            jax.ShapeDtypeStruct(stream.shape, bf16),
+            jax.ShapeDtypeStruct(conv_cache.shape, bf16),
+            jax.ShapeDtypeStruct(scan_state.shape, f32),
+        ),
+        in_specs=[pl.BlockSpec(memory_space=pl.ANY)] * len(arrays),
+        out_specs=(
+            pl.BlockSpec(memory_space=pltpu.VMEM),
+            pl.BlockSpec(memory_space=pl.ANY),
+            pl.BlockSpec(memory_space=pl.ANY),
+        ),
+        scratch_shapes=landing
+        + [
+            pltpu.VMEM(conv_cache.shape, bf16),
+            pltpu.VMEM((n * ROWS, LANES), f32),
+            pltpu.VMEM((n, ROWS, LANES), bf16),
+            pltpu.VMEM((n, ROWS, LANES), bf16),
+            pltpu.VMEM((n,) + tile, bf16),
+            pltpu.VMEM((blocks, LANES), bf16),
+            pltpu.VMEM((n, blocks, LANES), bf16),
+            pltpu.VMEM(tile, bf16),
+            pltpu.VMEM((n,) + tile, bf16),
+            pltpu.VMEM((n,) + tile, bf16),
+            pltpu.VMEM((n,) + tile, bf16),
+            pltpu.VMEM((1, LANES), f32),
+            pltpu.VMEM((n, 1, LANES), f32),
+            pltpu.VMEM((4 * 24, LANES), f32),
+            pltpu.VMEM((3 * 24, LANES), f32),
+            pltpu.VMEM((blocks, LANES), f32),
+            pltpu.VMEM((LANES, LANES), f32),
+            pltpu.VMEM((n * blocks, LANES), f32),
+            pltpu.VMEM((n,) + tile, bf16),
+            pltpu.SemaphoreType.DMA((len(arrays),)),
+            pltpu.SemaphoreType.DMA((2,)),
+            pltpu.SemaphoreType.DMA((6, n)),
+            pltpu.SemaphoreType.DMA((6, n)),
+        ],
+        compiler_params=pltpu.CompilerParams(
+            collective_id=0, has_side_effects=True, vmem_limit_bytes=40 * 1024 * 1024
+        ),
+    )(*arrays)
+
+
+def fits(arrays):
+    n = lax.axis_size("ep")
+    stream, conv_cache, scan_state = arrays[:3]
+    head_count, head_dim, state = scan_state.shape[1:]
+    blocks = arrays[3].shape[1] // LANES
+    groups = arrays[5].shape[1] // LANES
+    return (
+        stream.shape == (n, LANES)
+        and conv_cache.shape[0] == 1
+        and state == LANES
+        and LANES % head_dim == 0
+        and head_count <= LANES
+        and blocks % 8 == 0
+        and 2 * blocks <= LANES
+        and 2 * tokens_of(stream) <= LANES
+        and blocks % groups == 0
+        and arrays[8].shape[0] == 4
+        and blocks + 2 * groups < 24
+        and 2 * blocks + 2 * groups < ROWS
+    )
+
+
+def tokens_of(stream):
+    return stream.shape[0]
+
+
+def dispatch(*arrays):
+    if fits(arrays):
+        return fused(*arrays)
+    return on_device(*arrays)
+
+
 def solution(mesh):
     return jax.shard_map(
-        on_device,
+        dispatch,
         mesh=mesh,
         in_specs=(
             P("grp", "ep"),

time: 192 us -> 53.3 us (0.28)
  blocking collectives: 162 us -> 0 us
  Pallas kernels: 0 us -> 31.7 us
  local copies, waits for them, and re-layouts: 6.89 us -> 20 us
  matrix products: 9.08 us -> 0 us
  waiting for transfers between devices: 4.33 us -> 0 us
  other arithmetic: 4.32 us -> 0 us
  starting transfers between devices: 3.63 us -> 0 us
    unnamed x1 -> x0, blocking collectives: 66.2 us -> none
    psum x2 -> x0, blocking collectives: 61.1 us -> none  [the longest x1 31.4 us: on_device(): lax.psum((jnp.sum(residual, axis=1), jnp.sum(residual * residual, axis=1)...]
    all_gather x2 -> x0, blocking collectives: 34.6 us -> none  [the longest x1 17.3 us: on_device(): lax.all_gather(normed, 'ep', axis=0, tiled=True)]
    pallas_call x0 -> x1, Pallas kernels: none -> 31.7 us  [fused(): pl.pallas_call(functools.partial(fused_kernel, (n, inner, groups, scan_st...]
    unnamed x37 -> x48, local copies, waits for them, and re-layouts: 4.03 us -> 20 us
    dot_general x12 -> x0, matrix products: 9.08 us -> none  [the longest x5 4.26 us: on_device(): jnp.dot(stream, weight, preferred_element_type=jnp.float32)]
    all_to_all x1 -> x0, waiting for transfers between devices: 4.33 us -> none  [on_device(): lax.all_to_all(expert_out, 'ep', split_axis=1, concat_axis=0, tiled=True)]
    all_to_all x1 -> x0, starting transfers between devices: 3.63 us -> none  [on_device(): lax.all_to_all(expert_out, 'ep', split_axis=1, concat_axis=0, tiled=True)]
  transfers between devices with their start and end apart: 1 -> 0, of which waited for: 1 -> 0; matrix products, arithmetic and copies ran while one was open for 1% -> 0% of each run, Pallas kernels for 0% -> 0%
where the time goes in v1:
time: 53.3 us; the launch traced here: 52.4 us
  Pallas kernels  31.7 us (59%)
  local copies, waits for them, and re-layouts  20 us (38%)
  between operations  0.73 us (1%)
    pallas_call x1, Pallas kernels, fused(): pl.pallas_call(functools.partial(fused_kernel, (n, inner, groups, scan_st...  31.7 us
    unnamed x48, local copies, waits for them, and re-layouts  20 us

profile of v1, /device:TPU:0, one launch (start us, length us, event | category | flops | bytes accessed | tf_op | source)
XLA Modules:
  0.0 52.4 jit_solution(10995778348161432391)
XLA Ops:
  0.6 0.0 copy-start.10
  0.6 0.8 %copy.28.routes = s32[16,4]{1,0:T(8,128)S(1)} copy(s32[16,4]{0,1:T(4,128)} %param.39) | data formatting | bytes 512 | tf_op args[15]
  1.4 0.8 %copy.29.route_weight = f32[16,4]{1,0:T(8,128)S(1)} copy(f32[16,4]{0,1:T(4,128)} %param.40) | data formatting | bytes 512 | tf_op args[16]
  2.2 0.0 copy-start.16
  2.2 0.0 copy-start.20
  2.2 0.9 %copy.27.step_weight = bf16[128,32]{1,0:T(8,128)(2,1)S(1)} copy(bf16[128,32]{0,1:T(8,128)(2,1)} %param.31) | data formatting | bytes 16384 | tf_op args[7]
  3.1 0.0 copy-done.10
  3.1 0.0 copy-done.16
  3.1 0.0 copy-done.17
  3.1 0.0 copy-done.18
  3.1 0.0 copy-done.19
  3.1 0.0 copy-done.20
  3.1 0.0 copy-start
  3.1 1.2 %copy-done = f32[1,32,64,128]{3,2,1,0:T(8,128)S(1)} copy-done((f32[1,32,64,128]{3,2,1,0:T(8,128)S(1)}, f32[1,32,64,128]{3,2,1,0:T(8,128)}, u32[]{:S(2)}) %copy-start) | copy-done | bytes 1048600
  4.4 1.2 %copy-done.1 = bf16[1,2048,256]{2,1,0:T(8,128)(2,1)S(1)} copy-done((bf16[1,2048,256]{2,1,0:T(8,128)(2,1)S(1)}, bf16[1,2048,256]{2,1,0:T(8,128)(2,1)}, u32[]{:S(2)}) %copy-start.1) | copy-done | bytes 1048600
  5.6 1.2 %copy-done.2 = bf16[1,2048,256]{2,1,0:T(8,128)(2,1)S(1)} copy-done((bf16[1,2048,256]{2,1,0:T(8,128)(2,1)S(1)}, bf16[1,2048,256]{2,1,0:T(8,128)(2,1)}, u32[]{:S(2)}) %copy-start.2) | copy-done | bytes 1048600
  6.8 1.2 %copy-done.3 = bf16[1,256,2048]{2,1,0:T(8,128)(2,1)S(1)} copy-done((bf16[1,256,2048]{2,1,0:T(8,128)(2,1)S(1)}, bf16[1,256,2048]{2,1,0:T(8,128)(2,1)}, u32[]{:S(2)}) %copy-start.3) | copy-done | bytes 1048600
  8.0 1.2 %copy-done.4 = bf16[2048,256]{1,0:T(8,128)(2,1)S(1)} copy-done((bf16[2048,256]{1,0:T(8,128)(2,1)S(1)}, bf16[2048,256]{1,0:T(8,128)(2,1)}, u32[]{:S(2)}) %copy-start.4) | copy-done | bytes 1048600
  9.3 1.2 %copy-done.5 = bf16[2048,256]{1,0:T(8,128)(2,1)S(1)} copy-done((bf16[2048,256]{1,0:T(8,128)(2,1)S(1)}, bf16[2048,256]{1,0:T(8,128)(2,1)}, u32[]{:S(2)}) %copy-start.5) | copy-done | bytes 1048600
  10.5 1.2 %copy-done.6 = bf16[256,2048]{1,0:T(8,128)(2,1)S(1)} copy-done((bf16[256,2048]{1,0:T(8,128)(2,1)S(1)}, bf16[256,2048]{1,0:T(8,128)(2,1)}, u32[]{:S(2)}) %copy-start.6) | copy-done | bytes 1048600
  11.7 1.0 %copy-done.7 = bf16[128,2048]{1,0:T(8,128)(2,1)S(1)} copy-done((bf16[128,2048]{1,0:T(8,128)(2,1)S(1)}, bf16[128,2048]{1,0:T(8,128)(2,1)}, u32[]{:S(2)}) %copy-start.7) | copy-done | bytes 524312
  12.8 1.0 %copy-done.8 = bf16[128,2048]{1,0:T(8,128)(2,1)S(1)} copy-done((bf16[128,2048]{1,0:T(8,128)(2,1)S(1)}, bf16[128,2048]{1,0:T(8,128)(2,1)}, u32[]{:S(2)}) %copy-start.8) | copy-done | bytes 524312
  13.8 1.0 %copy-done.9 = bf16[2048,128]{1,0:T(8,128)(2,1)S(1)} copy-done((bf16[2048,128]{1,0:T(8,128)(2,1)S(1)}, bf16[2048,128]{1,0:T(8,128)(2,1)}, u32[]{:S(2)}) %copy-start.9) | copy-done | bytes 524312
  14.8 0.8 %copy-done.11 = bf16[128,256]{1,0:T(8,128)(2,1)S(1)} copy-done((bf16[128,256]{1,0:T(8,128)(2,1)S(1)}, bf16[128,256]{1,0:T(8,128)(2,1)}, u32[]{:S(2)}) %copy-start.11) | copy-done | bytes 65560
  15.7 0.7 %copy-done.12 = bf16[1,3,2560]{2,1,0:T(4,128)(2,1)S(1)} copy-done((bf16[1,3,2560]{2,1,0:T(4,128)(2,1)S(1)}, bf16[1,3,2560]{2,1,0:T(4,128)(2,1)}, u32[]{:S(2)}) %copy-start.12) | copy-done | bytes 15384
  16.4 0.7 %copy-done.13 = bf16[4,2560]{1,0:T(4,128)(2,1)S(1)} copy-done((bf16[4,2560]{1,0:T(4,128)(2,1)S(1)}, bf16[4,2560]{1,0:T(4,128)(2,1)}, u32[]{:S(2)}) %copy-start.13) | copy-done | bytes 20504
  17.1 0.7 %copy-done.14 = f32[2048]{0:T(1024)S(1)} copy-done((f32[2048]{0:T(1024)S(1)}, f32[2048]{0:T(1024)}, u32[]{:S(2)}) %copy-start.14) | copy-done | bytes 8216
  17.8 0.7 %copy-done.15 = f32[2048]{0:T(1024)S(1)} copy-done((f32[2048]{0:T(1024)S(1)}, f32[2048]{0:T(1024)}, u32[]{:S(2)}) %copy-start.15) | copy-done | bytes 8216
  18.5 31.7 %shard_map.247 = (bf16[16,128]{1,0:T(8,128)(2,1)S(1)}, bf16[1,3,2560]{2,1,0:T(4,128)(2,1)S(1)}, f32[1,32,64,128]{3,2,1,0:T(8,128)S(1)}) custom-call(bf16[16,128]{1,0:T(8,128)(2,1)S(1)} %copy-done.16, bf16[1,3,2560]{2,1,0:T(4,128)(2,1)S(1)} %copy-done.12, f32[1,32,64,128]{3,2,1,0:T(8,128)S(1)} %copy-done, bf16[128,2048]{1,0:T(8,128)(2,1)S(1)} %copy-done.7, ...), custom_call_target="tpu_custom_call" | custom-call | tf_op jit(solution)/shard_map/pallas_call | solution.py:563
  50.2 0.6 %copy.33 = bf16[16,128]{1,0:T(8,128)(2,1)} copy(bf16[16,128]{1,0:T(8,128)(2,1)S(1)} %get-tuple-element.6) | data formatting | bytes 8192
  50.8 0.6 %copy.34 = bf16[1,3,2560]{2,1,0:T(4,128)(2,1)} copy(bf16[1,3,2560]{2,1,0:T(4,128)(2,1)S(1)} %get-tuple-element.7) | data formatting | bytes 30720
  51.4 1.0 %copy.35 = f32[1,32,64,128]{3,2,1,0:T(8,128)} copy(f32[1,32,64,128]{3,2,1,0:T(8,128)S(1)} %get-tuple-element.8) | data formatting | bytes 2097152
  (17 shorter events, 0.0 us)
Async XLA Ops:
  0.6 2.4 %copy-start.10 = (bf16[128,256]{1,0:T(8,128)(2,1)S(1)}, bf16[128,256]{1,0:T(8,128)(2,1)}, u32[]{:S(2)}) copy-start(bf16[128,256]{1,0:T(8,128)(2,1)} %entry_weight.1) | copy-start | bytes 196612
  2.2 0.9 %copy-start.16 = (bf16[16,128]{1,0:T(8,128)(2,1)S(1)}, bf16[16,128]{1,0:T(8,128)(2,1)}, u32[]{:S(2)}) copy-start(bf16[16,128]{1,0:T(8,128)(2,1)} %stream.1) | copy-start | bytes 12292
  2.2 0.9 %copy-start.17 = (f32[32]{0:T(128)S(1)}, f32[32]{0:T(128)}, u32[]{:S(2)}) copy-start(f32[32]{0:T(128)} %param.33) | copy-start | bytes 388
  2.2 0.9 %copy-start.18 = (f32[32]{0:T(128)S(1)}, f32[32]{0:T(128)}, u32[]{:S(2)}) copy-start(f32[32]{0:T(128)} %param.34) | copy-start | bytes 388
  2.2 0.9 %copy-start.19 = (f32[32]{0:T(128)S(1)}, f32[32]{0:T(128)}, u32[]{:S(2)}) copy-start(f32[32]{0:T(128)} %param.35) | copy-start | bytes 388
  2.2 0.9 %copy-start.20 = (f32[128]{0:T(128)S(1)}, f32[128]{0:T(128)}, u32[]{:S(2)}) copy-start(f32[128]{0:T(128)} %param.47) | copy-start | bytes 1540
  3.1 1.2 %copy-start = (f32[1,32,64,128]{3,2,1,0:T(8,128)S(1)}, f32[1,32,64,128]{3,2,1,0:T(8,128)}, u32[]{:S(2)}) copy-start(f32[1,32,64,128]{3,2,1,0:T(8,128)} %scan_state.1) | copy-start | bytes 3145732
  4.4 1.2 %copy-start.1 = (bf16[1,2048,256]{2,1,0:T(8,128)(2,1)S(1)}, bf16[1,2048,256]{2,1,0:T(8,128)(2,1)}, u32[]{:S(2)}) copy-start(bf16[1,2048,256]{2,1,0:T(8,128)(2,1)} %expert_gate.1) | copy-start | bytes 3145732
  5.6 1.2 %copy-start.2 = (bf16[1,2048,256]{2,1,0:T(8,128)(2,1)S(1)}, bf16[1,2048,256]{2,1,0:T(8,128)(2,1)}, u32[]{:S(2)}) copy-start(bf16[1,2048,256]{2,1,0:T(8,128)(2,1)} %expert_up.1) | copy-start | bytes 3145732
  6.8 1.2 %copy-start.3 = (bf16[1,256,2048]{2,1,0:T(8,128)(2,1)S(1)}, bf16[1,256,2048]{2,1,0:T(8,128)(2,1)}, u32[]{:S(2)}) copy-start(bf16[1,256,2048]{2,1,0:T(8,128)(2,1)} %expert_down.1) | copy-start | bytes 3145732
  8.0 1.2 %copy-start.4 = (bf16[2048,256]{1,0:T(8,128)(2,1)S(1)}, bf16[2048,256]{1,0:T(8,128)(2,1)}, u32[]{:S(2)}) copy-start(bf16[2048,256]{1,0:T(8,128)(2,1)} %shared_gate.1) | copy-start | bytes 3145732
  9.3 1.2 %copy-start.5 = (bf16[2048,256]{1,0:T(8,128)(2,1)S(1)}, bf16[2048,256]{1,0:T(8,128)(2,1)}, u32[]{:S(2)}) copy-start(bf16[2048,256]{1,0:T(8,128)(2,1)} %shared_up.1) | copy-start | bytes 3145732
  10.5 1.2 %copy-start.6 = (bf16[256,2048]{1,0:T(8,128)(2,1)S(1)}, bf16[256,2048]{1,0:T(8,128)(2,1)}, u32[]{:S(2)}) copy-start(bf16[256,2048]{1,0:T(8,128)(2,1)} %shared_down.1) | copy-start | bytes 3145732
  11.7 1.0 %copy-start.7 = (bf16[128,2048]{1,0:T(8,128)(2,1)S(1)}, bf16[128,2048]{1,0:T(8,128)(2,1)}, u32[]{:S(2)}) copy-start(bf16[128,2048]{1,0:T(8,128)(2,1)} %gate_weight.1) | copy-start | bytes 1572868
  12.8 1.0 %copy-start.8 = (bf16[128,2048]{1,0:T(8,128)(2,1)S(1)}, bf16[128,2048]{1,0:T(8,128)(2,1)}, u32[]{:S(2)}) copy-start(bf16[128,2048]{1,0:T(8,128)(2,1)} %value_weight.1) | copy-start | bytes 1572868
  13.8 1.0 %copy-start.9 = (bf16[2048,128]{1,0:T(8,128)(2,1)S(1)}, bf16[2048,128]{1,0:T(8,128)(2,1)}, u32[]{:S(2)}) copy-start(bf16[2048,128]{1,0:T(8,128)(2,1)} %out_weight.1) | copy-start | bytes 1572868
  14.8 0.8 %copy-start.11 = (bf16[128,256]{1,0:T(8,128)(2,1)S(1)}, bf16[128,256]{1,0:T(8,128)(2,1)}, u32[]{:S(2)}) copy-start(bf16[128,256]{1,0:T(8,128)(2,1)} %readout_weight.1) | copy-start | bytes 196612
  15.7 0.7 %copy-start.12 = (bf16[1,3,2560]{2,1,0:T(4,128)(2,1)S(1)}, bf16[1,3,2560]{2,1,0:T(4,128)(2,1)}, u32[]{:S(2)}) copy-start(bf16[1,3,2560]{2,1,0:T(4,128)(2,1)} %conv_cache.1) | copy-start | bytes 46084
  16.4 0.7 %copy-start.13 = (bf16[4,2560]{1,0:T(4,128)(2,1)S(1)}, bf16[4,2560]{1,0:T(4,128)(2,1)}, u32[]{:S(2)}) copy-start(bf16[4,2560]{1,0:T(4,128)(2,1)} %conv_weight.1) | copy-start | bytes 61444
  17.1 0.7 %copy-start.14 = (f32[2048]{0:T(1024)S(1)}, f32[2048]{0:T(1024)}, u32[]{:S(2)}) copy-start(f32[2048]{0:T(1024)} %param.36) | copy-start | bytes 24580
  17.8 0.7 %copy-start.15 = (f32[2048]{0:T(1024)S(1)}, f32[2048]{0:T(1024)}, u32[]{:S(2)}) copy-start(f32[2048]{0:T(1024)} %param.38) | copy-start | bytes 24580

commit v2 on v1

--- a/solution.py
+++ b/solution.py
@@ -239,7 +239,6 @@
     s2_v,
     conv_v,
     stage,
-    part_send,
     part_recv,
     x_recv,
     norm_send,
@@ -338,10 +337,12 @@
         loads[index].wait()
     x = x_v[...]
     place = (iota((heads, LANES), 0) == iota((heads, LANES), 1)).astype(jnp.bfloat16)
-    step_wide = jnp.dot(ws_v[...], place, preferred_element_type=jnp.float32).astype(jnp.bfloat16)
+    step_wide = lax.dot_general(
+        place, ws_v[...], (((0,), (0,)), ((), ())), preferred_element_type=jnp.float32
+    ).astype(jnp.bfloat16)
     base = 2 * blocks + 2 * groups
-    stage[pl.ds(base, tokens, stride=ROWS), :] = jnp.dot(
-        x, step_wide, preferred_element_type=jnp.float32
+    stage[pl.ds(base, tokens, stride=ROWS), :] = lax.dot_general(
+        x, step_wide, (((1,), (1,)), ((), ())), preferred_element_type=jnp.float32
     )
     for extra in range(base + 1, ROWS):
         stage[pl.ds(extra, tokens, stride=ROWS), :] = jnp.zeros((tokens, LANES), jnp.float32)
@@ -354,11 +355,8 @@
                 :, j * LANES : (j + 1) * LANES
             ]
         base += ref.shape[1] // LANES
-    for t in range(tokens):
-        part_send[t] = stage[t * ROWS : (t + 1) * ROWS, :].astype(jnp.bfloat16)
     pl.semaphore_wait(barrier, n - 1)
-    post(0, lambda peer: part_send.at[peer], part_recv)
-    post(1, lambda peer: x_v, x_recv)
+    post(0, lambda peer: stage.at[pl.ds(pl.multiple_of(peer * ROWS, ROWS), ROWS)], part_recv)
 
     for index in range(6, 16):
         loads[index].wait()
@@ -397,7 +395,8 @@
     total = stage[pl.ds(pl.multiple_of(me * ROWS, ROWS), ROWS), :]
     for k in range(1, n):
         sender = arrive(0, part_recv, k)
-        total = total + part_recv[sender].astype(jnp.float32)
+        total = total + part_recv[sender]
+    post(1, lambda peer: x_v, x_recv)
     total = total.astype(jnp.bfloat16).astype(jnp.float32)
     fresh = total[blocks : blocks + 24, :]
     active = silu(before + fresh * last_tap)
@@ -472,7 +471,9 @@
     mix_send[...] = mixed
     post(3, lambda peer: mix_send, mix_recv)
     mix_recv[me] = mixed
-    mine = jnp.sum(jnp.where(rt_v[...] == me, rw_v[...], 0.0), axis=1, keepdims=True)
+    mine = jnp.sum(jnp.where(rt_v[...] == me, rw_v[...], 0.0), axis=0, keepdims=True)
+    same = iota((tokens, tokens), 0) == iota((tokens, tokens), 1)
+    mine = jnp.sum(jnp.where(same, mine, 0.0), axis=1, keepdims=True)
     for k in range(1, n):
         arrive(3, mix_recv, k)
 
@@ -545,11 +546,14 @@
 
 def fused(*arrays):
     (stream, conv_cache, scan_state) = arrays[:3]
+    conv_weight = arrays[8]
     n = lax.axis_size("ep")
     inner = arrays[3].shape[1]
     groups = arrays[5].shape[1] // scan_state.shape[3]
     blocks = inner // LANES
     arrays = [a.reshape(1, -1) if a.ndim == 1 else a for a in arrays]
+    for index in (7, 15, 16):
+        arrays[index] = arrays[index].T
     tile = (stream.shape[0], LANES)
     landing = []
     for index, a in enumerate(arrays):
@@ -567,7 +571,7 @@
             jax.ShapeDtypeStruct(conv_cache.shape, bf16),
             jax.ShapeDtypeStruct(scan_state.shape, f32),
         ),
-        in_specs=[pl.BlockSpec(memory_space=pl.ANY)] * len(arrays),
+        in_specs=[pl.BlockSpec(memory_space=pltpu.HBM)] * len(arrays),
         out_specs=(
             pl.BlockSpec(memory_space=pltpu.VMEM),
             pl.BlockSpec(memory_space=pl.ANY),
@@ -577,8 +581,7 @@
         + [
             pltpu.VMEM(conv_cache.shape, bf16),
             pltpu.VMEM((n * ROWS, LANES), f32),
-            pltpu.VMEM((n, ROWS, LANES), bf16),
-            pltpu.VMEM((n, ROWS, LANES), bf16),
+            pltpu.VMEM((n, ROWS, LANES), f32),
             pltpu.VMEM((n,) + tile, bf16),
             pltpu.VMEM((blocks, LANES), bf16),
             pltpu.VMEM((n, blocks, LANES), bf16),
@@ -588,8 +591,8 @@
             pltpu.VMEM((n,) + tile, bf16),
             pltpu.VMEM((1, LANES), f32),
             pltpu.VMEM((n, 1, LANES), f32),
-            pltpu.VMEM((4 * 24, LANES), f32),
-            pltpu.VMEM((3 * 24, LANES), f32),
+            pltpu.VMEM((conv_weight.shape[0] * 24, LANES), f32),
+            pltpu.VMEM((conv_cache.shape[1] * 24, LANES), f32),
             pltpu.VMEM((blocks, LANES), f32),
             pltpu.VMEM((LANES, LANES), f32),
             pltpu.VMEM((n * blocks, LANES), f32),
@@ -600,7 +603,7 @@
             pltpu.SemaphoreType.DMA((6, n)),
         ],
         compiler_params=pltpu.CompilerParams(
-            collective_id=0, has_side_effects=True, vmem_limit_bytes=40 * 1024 * 1024
+            collective_id=0, has_side_effects=True, vmem_limit_bytes=67043328
         ),
     )(*arrays)
 
@@ -621,7 +624,7 @@
         and 2 * blocks <= LANES
         and 2 * tokens_of(stream) <= LANES
         and blocks % groups == 0
-        and arrays[8].shape[0] == 4
+        and arrays[8].shape[0] == conv_cache.shape[1] + 1
         and blocks + 2 * groups < 24
         and 2 * blocks + 2 * groups < ROWS
     )

time: 53.3 us -> 41.3 us (0.77); the launches traced: 52.4 us -> 41 us
  local copies, waits for them, and re-layouts: 20 us -> 4.91 us
  Pallas kernels: 31.7 us -> 35.5 us
    unnamed x48 -> x5, local copies, waits for them, and re-layouts: 20 us -> 4.91 us
    pallas_call x1, Pallas kernels: 31.7 us -> 35.5 us  [fused(): pl.pallas_call(functools.partial(fused_kernel, (n, inner, groups, scan_st...]
where the time goes in v2:
time: 41.3 us; the launch traced here: 41 us
  Pallas kernels  35.5 us (86%)
  local copies, waits for them, and re-layouts  4.91 us (12%)
  between operations  0.66 us (2%)
    pallas_call x1, Pallas kernels, fused(): pl.pallas_call(functools.partial(fused_kernel, (n, inner, groups, scan_st...  35.5 us
    unnamed x5, local copies, waits for them, and re-layouts  4.91 us

profile of v2, /device:TPU:0, one launch (start us, length us, event | category | flops | bytes accessed | tf_op | source)
XLA Modules:
  0.0 41.0 jit_solution(1197206423167377606)
XLA Ops:
  0.6 35.5 %shard_map.247 = (bf16[16,128]{1,0:T(8,128)(2,1)}, bf16[1,3,2560]{2,1,0:T(4,128)(2,1)}, f32[1,32,64,128]{3,2,1,0:T(8,128)}) custom-call(bf16[16,128]{1,0:T(8,128)(2,1)} %stream.1, bf16[1,3,2560]{2,1,0:T(4,128)(2,1)} %conv_cache.1, f32[1,32,64,128]{3,2,1,0:T(8,128)} %scan_state.1, bf16[128,2048]{1,0:T(8,128)(2,1)} %gate_weight.1, ...), custom_call_target="tpu_custom_call" | custom-call | tf_op jit(solution)/shard_map/pallas_call | solution.py:567
  36.1 0.0 copy-start
  36.1 0.7 %copy-done = bf16[16,128]{1,0:T(8,128)(2,1)S(1)} copy-done((bf16[16,128]{1,0:T(8,128)(2,1)S(1)}, bf16[16,128]{1,0:T(8,128)(2,1)}, u32[]{:S(2)}) %copy-start) | copy-done | bytes 4120
  36.8 0.6 %copy.30 = bf16[16,128]{1,0:T(8,128)(2,1)} copy(bf16[16,128]{1,0:T(8,128)(2,1)S(1)} %copy-done) | data formatting | bytes 8192
  37.4 1.3 %copy.31 = bf16[1,3,2560]{2,1,0:T(4,128)(2,1)} copy(bf16[1,3,2560]{2,1,0:T(4,128)(2,1)} %get-tuple-element.7) | data formatting | bytes 30720
  38.7 2.3 %copy.32 = f32[1,32,64,128]{3,2,1,0:T(8,128)} copy(f32[1,32,64,128]{3,2,1,0:T(8,128)} %get-tuple-element.8) | data formatting | bytes 2097152
Async XLA Ops:
  36.1 0.7 %copy-start = (bf16[16,128]{1,0:T(8,128)(2,1)S(1)}, bf16[16,128]{1,0:T(8,128)(2,1)}, u32[]{:S(2)}) copy-start(bf16[16,128]{1,0:T(8,128)(2,1)} %get-tuple-element.6) | copy-start | bytes 12292

commit v3 on v2

--- a/solution.py
+++ b/solution.py
@@ -239,6 +239,7 @@
     s2_v,
     conv_v,
     stage,
+    pair_recv,
     part_recv,
     x_recv,
     norm_send,
@@ -307,8 +308,8 @@
 
     pending = []
 
-    def post(phase, source, target):
-        for k in range(1, n):
+    def post(phase, source, target, stride=1):
+        for k in range(stride, n, stride):
             peer = lax.rem(me + k, n)
             copy = pltpu.make_async_remote_copy(
                 src_ref=source(peer),
@@ -356,7 +357,28 @@
             ]
         base += ref.shape[1] // LANES
     pl.semaphore_wait(barrier, n - 1)
-    post(0, lambda peer: stage.at[pl.ds(pl.multiple_of(peer * ROWS, ROWS), ROWS)], part_recv)
+    def token_rows(token):
+        return pl.ds(pl.multiple_of(token * ROWS, ROWS), ROWS)
+
+    parity = lax.rem(me, 2)
+    exchanges = []
+    for k in range(n // 2):
+        copy = pltpu.make_async_remote_copy(
+            src_ref=stage.at[token_rows(2 * k + 1 - parity)],
+            dst_ref=pair_recv.at[k],
+            send_sem=send_sem.at[6, k],
+            recv_sem=recv_sem.at[6, k],
+            device_id={"ep": me + 1 - 2 * parity},
+            device_id_type=MESH,
+        )
+        copy.start()
+        exchanges.append(copy)
+        pending.append(copy)
+    for k in range(n // 2):
+        exchanges[k].wait_recv()
+        own_rows = token_rows(2 * k + parity)
+        stage[own_rows, :] = stage[own_rows, :] + pair_recv[k]
+    post(0, lambda peer: stage.at[token_rows(peer)], part_recv, 2)
 
     for index in range(6, 16):
         loads[index].wait()
@@ -392,8 +414,8 @@
     last_tap = taps[(tap_count - 1) * 24 : tap_count * 24, :]
     loads[16].wait()
 
-    total = stage[pl.ds(pl.multiple_of(me * ROWS, ROWS), ROWS), :]
-    for k in range(1, n):
+    total = stage[token_rows(me), :]
+    for k in range(2, n, 2):
         sender = arrive(0, part_recv, k)
         total = total + part_recv[sender]
     post(1, lambda peer: x_v, x_recv)
@@ -544,6 +566,42 @@
     conv_out.wait()
 
 
+CHUNKS = 4
+
+
+def deliver(
+    result_in,
+    conv_in,
+    state_in,
+    result_out,
+    conv_out,
+    state_out,
+    result_v,
+    conv_v,
+    state_v,
+    in_sem,
+    out_sem,
+):
+    size = state_in.shape[1] // CHUNKS
+    triples = [
+        tuple([r.at[0, pl.ds(c * size, size)] for r in (state_in, state_v, state_out)])
+        for c in range(CHUNKS)
+    ] + [(result_in, result_v, result_out), (conv_in, conv_v, conv_out)]
+    reads = [
+        pltpu.make_async_copy(a, v, in_sem.at[i]) for i, (a, v, _) in enumerate(triples)
+    ]
+    writes = [
+        pltpu.make_async_copy(v, b, out_sem.at[i]) for i, (_, v, b) in enumerate(triples)
+    ]
+    for read in reads:
+        read.start()
+    for read, write in zip(reads, writes):
+        read.wait()
+        write.start()
+    for write in writes:
+        write.wait()
+
+
 def fused(*arrays):
     (stream, conv_cache, scan_state) = arrays[:3]
     conv_weight = arrays[8]
@@ -564,7 +622,7 @@
             shape = (shape[0], LANES)
         landing.append(pltpu.VMEM(shape, a.dtype))
     bf16, f32 = jnp.bfloat16, jnp.float32
-    return pl.pallas_call(
+    outs = pl.pallas_call(
         functools.partial(fused_kernel, (n, inner, groups, scan_state.shape[2])),
         out_shape=(
             jax.ShapeDtypeStruct(stream.shape, bf16),
@@ -581,6 +639,7 @@
         + [
             pltpu.VMEM(conv_cache.shape, bf16),
             pltpu.VMEM((n * ROWS, LANES), f32),
+            pltpu.VMEM((n // 2, ROWS, LANES), f32),
             pltpu.VMEM((n, ROWS, LANES), f32),
             pltpu.VMEM((n,) + tile, bf16),
             pltpu.VMEM((blocks, LANES), bf16),
@@ -599,13 +658,22 @@
             pltpu.VMEM((n,) + tile, bf16),
             pltpu.SemaphoreType.DMA((len(arrays),)),
             pltpu.SemaphoreType.DMA((2,)),
-            pltpu.SemaphoreType.DMA((6, n)),
-            pltpu.SemaphoreType.DMA((6, n)),
+            pltpu.SemaphoreType.DMA((7, n)),
+            pltpu.SemaphoreType.DMA((7, n)),
         ],
         compiler_params=pltpu.CompilerParams(
             collective_id=0, has_side_effects=True, vmem_limit_bytes=67043328
         ),
     )(*arrays)
+    return pl.pallas_call(
+        deliver,
+        out_shape=tuple(jax.ShapeDtypeStruct(a.shape, a.dtype) for a in outs),
+        in_specs=[pl.BlockSpec(memory_space=pl.ANY)] * 3,
+        out_specs=(pl.BlockSpec(memory_space=pl.ANY),) * 3,
+        scratch_shapes=[pltpu.VMEM(a.shape, a.dtype) for a in outs]
+        + [pltpu.SemaphoreType.DMA((2 + CHUNKS,)), pltpu.SemaphoreType.DMA((2 + CHUNKS,))],
+        compiler_params=pltpu.CompilerParams(vmem_limit_bytes=67043328),
+    )(*outs)
 
 
 def fits(arrays):
@@ -616,6 +684,8 @@
     groups = arrays[5].shape[1] // LANES
     return (
         stream.shape == (n, LANES)
+        and n % 2 == 0
+        and head_count % CHUNKS == 0
         and conv_cache.shape[0] == 1
         and state == LANES
         and LANES % head_dim == 0

time: 41.3 us -> 36.4 us (0.88)
  local copies, waits for them, and re-layouts: 4.91 us -> 0 us
    unnamed x5 -> x0, local copies, waits for them, and re-layouts: 4.91 us -> none
    pallas_call x0 -> x1, Pallas kernels: none -> 2.02 us  [fused(): pl.pallas_call(deliver, out_shape=tuple((jax.ShapeDtypeStruct(a.shape, a....]
    pallas_call x1, Pallas kernels: 35.5 us -> 33.5 us  [fused(): pl.pallas_call(functools.partial(fused_kernel, (n, inner, groups, scan_st...]
where the time goes in v3:
time: 36.4 us; the launch traced here: 36.2 us
  Pallas kernels  35.5 us (98%)
  between operations  0.65 us (2%)
    pallas_call x1, Pallas kernels, fused(): pl.pallas_call(functools.partial(fused_kernel, (n, inner, groups, scan_st...  33.5 us
    pallas_call x1, Pallas kernels, fused(): pl.pallas_call(deliver, out_shape=tuple((jax.ShapeDtypeStruct(a.shape, a....  2.02 us

profile of v3, /device:TPU:0, one launch (start us, length us, event | category | flops | bytes accessed | tf_op | source)
XLA Modules:
  0.0 36.2 jit_solution(2275420517773740387)
XLA Ops:
  0.6 33.5 %shard_map.247 = (bf16[16,128]{1,0:T(8,128)(2,1)}, bf16[1,3,2560]{2,1,0:T(4,128)(2,1)}, f32[1,32,64,128]{3,2,1,0:T(8,128)}) custom-call(bf16[16,128]{1,0:T(8,128)(2,1)} %stream.1, bf16[1,3,2560]{2,1,0:T(4,128)(2,1)} %conv_cache.1, f32[1,32,64,128]{3,2,1,0:T(8,128)} %scan_state.1, bf16[128,2048]{1,0:T(8,128)(2,1)} %gate_weight.1, ...), custom_call_target="tpu_custom_call" | custom-call | tf_op jit(solution)/shard_map/pallas_call | solution.py:625
  34.2 2.0 %shard_map.248 = (bf16[16,128]{1,0:T(8,128)(2,1)}, bf16[1,3,2560]{2,1,0:T(4,128)(2,1)}, f32[1,32,64,128]{3,2,1,0:T(8,128)}) custom-call(bf16[16,128]{1,0:T(8,128)(2,1)} %get-tuple-element.6.result_in, bf16[1,3,2560]{2,1,0:T(4,128)(2,1)} %get-tuple-element.7.conv_in, f32[1,32,64,128]{3,2,1,0:T(8,128)} %get-tuple-element.8.state_in), custom_call_target="tpu_custom_call" | custom-call | tf_op jit(solution)/shard_map/pallas_call | solution.py:668
